TPU v7x, 32 devices: a whole 2x2x4 slice. The times are simulated.
32 devices in a mesh: ep: 16 (over z, y, x), tp: 2 (over core).
Axes of the slice: x: 2, y: 2, z: 4, core: 2. Of those that a mesh axis runs over, the one named last changes fastest.
Arguments:
- tokens: bfloat16 [192, 2048], P('ep', 'tp'), may hold values from -21 to 21
- norm_gain: bfloat16 [2048], P('tp'), may hold values from 0.099609375 to 1.8984375
- expert_ids: int32 [192, 8], P('ep'), may hold values from 0 to 31, all different within a row; in each aligned block of 12 rows (0 to 11, 12 to 23, ...) at most 5 rows name the same one
- route_gate: float32 [192, 8], P('ep'), may hold values from 0.05 to 1
- w_gate: bfloat16 [32, 2048, 512], P('ep', None, 'tp'), may hold values from -0.125 to 0.125
- w_up: bfloat16 [32, 2048, 512], P('ep', None, 'tp'), may hold values from -0.125 to 0.125
- w_down: bfloat16 [32, 512, 2048], P('ep', 'tp'), may hold values from -0.25 to 0.25
- shared_gate: bfloat16 [2048, 512], P(None, 'tp'), may hold values from -0.125 to 0.125
- shared_up: bfloat16 [2048, 512], P(None, 'tp'), may hold values from -0.125 to 0.125
- shared_down: bfloat16 [512, 2048], P('tp'), may hold values from -0.25 to 0.25
Outputs:
- mixed: bfloat16 [192, 2048], P('ep', 'tp')
Inputs may be any that keep to these rules, and one draw needn't show every extreme that they name: `expert_ids`: each row names 8 different experts; among the 12 rows of one device no expert is named more than once.
All inputs are finite; a program needn't handle non-finite values.
Results may differ from a plain program's by a relative error of at most 0.012.
Values may be sent and summed in bfloat16 or wider, within the bound.
A program may use at most 64 MiB of HBM per device.

v0:
```python
import jax
import jax.numpy as jnp
from jax import lax
from jax.sharding import PartitionSpec as P

D = 2048


eps = 1e-06
routed_scale = 2.5


def ranks_within(block_ids):
    count = block_ids.shape[-1]
    position = lax.iota(jnp.int32, count)
    equal_ids = block_ids[..., :, None] == block_ids[..., None, :]
    earlier = position[None, :] < position[:, None]
    return jnp.sum(equal_ids & earlier, axis=-1)


def apply_experts(inputs, w_gate, w_up, w_down):
    gate_value = jnp.einsum("sjcd,jdf->sjcf", inputs, w_gate, preferred_element_type=jnp.float32)
    up_value = jnp.einsum("sjcd,jdf->sjcf", inputs, w_up, preferred_element_type=jnp.float32)
    hidden = (jax.nn.silu(gate_value) * up_value).astype(jnp.bfloat16)
    partial_value = jnp.einsum(
        "sjcf,jfd->sjcd", hidden, w_down, preferred_element_type=jnp.float32
    ).astype(jnp.bfloat16)
    summed = lax.psum_scatter(partial_value, "tp", scatter_dimension=3, tiled=True).astype(
        jnp.float32
    )
    return summed.astype(jnp.bfloat16)


def send_back(results):
    return lax.all_to_all(results, "ep", split_axis=0, concat_axis=0, tiled=True)


def local(
    tokens,
    norm_gain,
    expert_ids,
    route_gate,
    w_gate,
    w_up,
    w_down,
    shared_gate,
    shared_up,
    shared_down,
):
    values = tokens.astype(jnp.float32)
    total_squares = lax.psum(jnp.sum(values * values, axis=-1), "tp")
    scale_rows = lax.rsqrt(total_squares / D + eps)[:, None]
    normed_part = (values * scale_rows * norm_gain.astype(jnp.float32)).astype(jnp.bfloat16)
    normed = lax.all_gather(normed_part, "tp", axis=1, tiled=True)
    weight = route_gate / jnp.sum(route_gate, axis=-1, keepdims=True) * routed_scale
    tok_dev = tokens.shape[0]
    top_count = expert_ids.shape[1]
    exp_dev = w_gate.shape[0]
    n_ep = lax.axis_size("ep")
    experts = exp_dev * n_ep
    capacity = (tok_dev * top_count * 3 // 2 + experts - 1) // experts
    ranking = ranks_within(expert_ids.reshape(tok_dev * top_count)).reshape(tok_dev, top_count)
    slot = expert_ids * capacity + ranking
    slot_count = experts * capacity
    matches = slot[None, :, :] == lax.iota(jnp.int32, slot_count)[:, None, None]
    selector = jnp.any(matches, axis=2).astype(jnp.bfloat16)
    outgoing = jnp.dot(selector, normed, preferred_element_type=jnp.float32).astype(jnp.bfloat16)
    outgoing = outgoing.reshape(n_ep, exp_dev, capacity, normed.shape[1])
    returned = send_back(
        apply_experts(
            lax.all_to_all(outgoing, "ep", split_axis=0, concat_axis=0, tiled=True),
            w_gate,
            w_up,
            w_down,
        )
    )
    returned = returned.reshape(slot_count, returned.shape[3])
    picked = returned[slot]
    routed = jnp.sum(picked.astype(jnp.float32) * weight[:, :, None], axis=1)
    gate_value = jnp.dot(normed, shared_gate, preferred_element_type=jnp.float32)
    up_value = jnp.dot(normed, shared_up, preferred_element_type=jnp.float32)
    shared_hidden = (jax.nn.silu(gate_value) * up_value).astype(jnp.bfloat16)
    shared_part = jnp.dot(shared_hidden, shared_down, preferred_element_type=jnp.float32)
    shared = lax.psum_scatter(
        shared_part.astype(jnp.bfloat16), "tp", scatter_dimension=1, tiled=True
    ).astype(jnp.float32)
    return (routed + shared).astype(jnp.bfloat16)


def solution(mesh):
    in_specs = (
        P("ep", "tp"),
        P("tp"),
        P("ep", None),
        P("ep", None),
        P("ep", None, "tp"),
        P("ep", None, "tp"),
        P("ep", "tp", None),
        P(None, "tp"),
        P(None, "tp"),
        P("tp", None),
    )
    out_specs = P("ep", "tp")
    return jax.shard_map(local, mesh=mesh, in_specs=in_specs, out_specs=out_specs, check_vma=False)
```

profile of v0, /device:TPU:0, one launch (start us, length us, event | category | flops | bytes accessed | tf_op | source)
XLA Modules:
  0.0 85.4 jit_solution(9204585525089918695)
XLA Ops:
  6.5 1.0 %fusion.32 = f32[12]{0:T(128)S(1)} fusion(bf16[12,1024]{1,0:T(8,128)(2,1)} %param.10), kind=kLoop, calls=%fused_computation.30 | loop fusion | flops 36852 | bytes 24624 | tf_op jit(solution)/shard_map/reduce_sum | solution.py:51
  7.6 2.6 %psum.7 = f32[12]{0:T(128)S(1)} all-reduce(f32[12]{0:T(128)S(1)} %fusion.32), channel_id=1, replica_groups=mesh['ep'=16,'tp'=2] {'tp'}, use_global_device_ids=true, to_apply=%region_3.0 | all-reduce | flops 12 | bytes 96 | tf_op jit(solution)/shard_map/psum | solution.py:51
  10.2 0.7 convert_element_type.44
  10.9 0.8 copy.34
  12.0 0.6 compare_select_fusion
  12.7 0.8 fusion.34
  13.6 1.8 %all_gather.3 = bf16[12,2048]{1,0:T(8,128)(2,1)S(1)} all-gather(bf16[12,1024]{1,0:T(8,128)(2,1)S(1)} %fusion.34), channel_id=1, replica_groups=mesh['ep'=16,'tp'=2] {'tp'}, dimensions={1}, use_global_device_ids=true | all-gather | bytes 73728 | tf_op jit(solution)/shard_map/all_gather | solution.py:54
  15.4 1.2 %convolution_convert_fusion.1 = bf16[160,2048]{1,0:T(8,128)(2,1)} fusion(pred[160,12]{0,1:T(8,128)(4,1)S(1)} %fusion.30, bf16[12,2048]{1,0:T(8,128)(2,1)S(1)} %all_gather.3), kind=kOutput, calls=%fused_computation.2 | convolution fusion | flops 8192000 | bytes 706432 | tf_op jit(solution)/shard_map/dot_general | solution.py:67
  16.6 1.3 %reshape.17 = bf16[16,2,5,2048]{3,2,1,0:T(8,128)(2,1)S(1)} reshape(bf16[160,2048]{1,0:T(8,128)(2,1)} %convolution_convert_fusion.1) | data formatting | bytes 1310720 | tf_op jit(solution)/shard_map/reshape | solution.py:68
  18.0 0.7 copy.36
  18.7 27.1 %all_to_all.10 = bf16[16,2,5,2048]{3,1,2,0:T(2,128)(2,1)S(1)} all-to-all(bf16[16,2,5,2048]{3,1,2,0:T(2,128)(2,1)S(1)} %copy.36), channel_id=1, replica_groups=mesh['ep'=16,'tp'=2] {'ep'}, dimensions={0} | all-to-all | bytes 1310720 | tf_op jit(solution)/shard_map/all_to_all | solution.py:71
  45.8 0.5 fusion.6
  46.3 3.3 %fusion = bf16[16,2,5,2048]{3,0,2,1:T(8,128)(2,1)} fusion(bf16[2,256,2048]{2,1,0:T(8,128)(2,1)S(1)} %copy-done, bf16[2,2048,256]{2,1,0:T(8,128)(2,1)} %param.15, bf16[16,2,5,2048]{3,1,2,0:T(2,128)(2,1)S(1)} %all_to_all.10, f32[16,2,5,256]{3,0,2,1:T(8,128)S(1)} %fusion.6), kind=kOutput, calls=%fused_computation.3 | convolution fusion | flops 336117760 | bytes 5668864 | tf_op jit(solution)/shard_map/sjcf,jfd->sjcd/dot_general | solution.py:25
  49.7 1.6 %fusion.44 = f32[12,256]{1,0:T(8,128)S(1)} fusion(bf16[12,2048]{1,0:T(8,128)(2,1)S(1)} %all_gather.3, bf16[2048,256]{1,0:T(8,128)(2,1)} %param.17), kind=kOutput, calls=%fused_computation.50 | convolution fusion | flops 12582912 | bytes 1110016 | tf_op jit(solution)/shard_map/dot_general | solution.py:80
  51.2 4.1 %reduce-scatter.3.cloned.1.call-done = bf16[16,2,5,1024]{3,0,2,1:T(8,128)(2,1)} async-done(((bf16[16,2,5,2048]{3,0,2,1:T(8,128)(2,1)}), bf16[16,2,5,1024]{3,0,2,1:T(8,128)(2,1)}) %reduce-scatter.3.cloned.1.call-update) | async-done | bytes 327696 | tf_op jit(solution)/shard_map/reduce_scatter | solution.py:28
  55.3 2.0 %copy.39 = bf16[16,2,5,1024]{3,1,2,0:T(2,128)(2,1)} copy(bf16[16,2,5,1024]{3,0,2,1:T(8,128)(2,1)} %reduce-scatter.3.cloned.1.call-done) | data formatting | bytes 655360 | tf_op jit(solution)/shard_map/reduce_scatter | solution.py:28
  57.4 6.7 %all-to-all-start.1 = ((bf16[16,2,5,1024]{3,1,2,0:T(2,128)(2,1)}), bf16[16,2,5,1024]{3,1,2,0:T(2,128)(2,1)S(1)}, u32[]{:S(2)}, u32[]{:S(2)}) async-start(bf16[16,2,5,1024]{3,1,2,0:T(2,128)(2,1)} %copy.39), calls=%async_computation.2 | async-start | bytes 655360 | tf_op jit(solution)/shard_map/all_to_all | solution.py:35
  64.2 2.6 %convolution_convert_fusion.2 = bf16[12,2048]{1,0:T(8,128)(2,1)} fusion(bf16[256,2048]{1,0:T(8,128)(2,1)S(1)} %copy-done.2, bf16[12,2048]{1,0:T(8,128)(2,1)S(1)} %all_gather.3, bf16[2048,256]{1,0:T(8,128)(2,1)} %param.18, f32[12,256]{1,0:T(8,128)S(1)} %fusion.44), kind=kOutput, calls=%fused_computation.4 | convolution fusion | flops 25208832 | bytes 2207744 | tf_op jit(solution)/shard_map/dot_general | solution.py:83
  66.8 0.7 reduce_sum.38
  67.5 0.7 divide_multiply_fusion
  68.3 0.8 reshape.21
  69.1 6.9 %all-to-all-done.1 = bf16[16,2,5,1024]{3,1,2,0:T(2,128)(2,1)S(1)} async-done(((bf16[16,2,5,1024]{3,1,2,0:T(2,128)(2,1)}), bf16[16,2,5,1024]{3,1,2,0:T(2,128)(2,1)S(1)}, u32[]{:S(2)}, u32[]{:S(2)}) %all-to-all-start.1) | async-done | bytes 327712 | tf_op jit(solution)/shard_map/all_to_all | solution.py:35
  76.2 0.8 gather_fusion
  77.2 1.4 %add_convert_fusion = bf16[12,1024]{1,0:T(8,128)(2,1)} fusion(f32[12,1024]{1,0:T(8,128)S(1)} %fusion.24, bf16[12,1024]{1,0:T(8,128)(2,1)} %reduce-scatter.5.cloned.1.call-done), kind=kLoop, calls=%fused_computation.33 | loop fusion | flops 36864 | bytes 98304 | tf_op jit(solution)/shard_map/convert_element_type | solution.py:87
  (21 shorter events, 1.1 us)
Async XLA Ops:
  6.5 39.7 %copy-start = (bf16[2,256,2048]{2,1,0:T(8,128)(2,1)S(1)}, bf16[2,256,2048]{2,1,0:T(8,128)(2,1)}, u32[]{:S(2)}) copy-start(bf16[2,256,2048]{2,1,0:T(8,128)(2,1)} %param.16) | copy-start | bytes 6291460
  6.5 48.8 %reduce-scatter.3.cloned.1.call-start = ((), (), s32[]{:S(2)}) async-start(), calls=%async_computation.4 | async-start | bytes 983040 | tf_op jit(solution)/shard_map/reduce_scatter | solution.py:28
  18.0 27.8 %copy-start.1 = (bf16[2,2048,256]{2,1,0:T(8,128)(2,1)S(1)}, bf16[2,2048,256]{2,1,0:T(8,128)(2,1)}, u32[]{:S(2)}) copy-start(bf16[2,2048,256]{2,1,0:T(8,128)(2,1)} %param.14) | copy-start | bytes 6291460
  49.6 14.5 %copy-start.2 = (bf16[256,2048]{1,0:T(8,128)(2,1)S(1)}, bf16[256,2048]{1,0:T(8,128)(2,1)}, u32[]{:S(2)}) copy-start(bf16[256,2048]{1,0:T(8,128)(2,1)} %param.19) | copy-start | bytes 3145732
  57.4 18.6 %all-to-all-start.1 = ((bf16[16,2,5,1024]{3,1,2,0:T(2,128)(2,1)}), bf16[16,2,5,1024]{3,1,2,0:T(2,128)(2,1)S(1)}, u32[]{:S(2)}, u32[]{:S(2)}) async-start(bf16[16,2,5,1024]{3,1,2,0:T(2,128)(2,1)} %copy.39), calls=%async_computation.2 | async-start | bytes 655360 | tf_op jit(solution)/shard_map/all_to_all | solution.py:35
  64.1 13.1 %reduce-scatter.5.cloned.1.call-start = ((), (), s32[]{:S(2)}) async-start(), calls=%async_computation.5 | async-start | bytes 98304 | tf_op jit(solution)/shard_map/reduce_scatter | solution.py:84
Sparse Core Ops, SparseCore 0:
  49.8 5.5 reduce-scatter.2
  67.1 8.8 reduce-scatter.4
where the time goes:
time: 86.1 us; the launch traced here: 85.4 us
  blocking collectives  31.5 us (37%)
  between operations  13.5 us (16%)
  waiting for transfers between devices  11 us (13%)
  matrix products  9.17 us (11%)
  local copies, waits for them, and re-layouts  6.95 us (8%)
  starting transfers between devices  6.78 us (8%)
  other arithmetic  6.44 us (7%)
    all_to_all x1, blocking collectives, local(): lax.all_to_all(outgoing, 'ep', split_axis=0, concat_axis=0, tiled=True)  27.1 us
    all_to_all x1, waiting for transfers between devices, send_back(): lax.all_to_all(results, 'ep', split_axis=0, concat_axis=0, tiled=True)  6.86 us
    all_to_all x1, starting transfers between devices, send_back(): lax.all_to_all(results, 'ep', split_axis=0, concat_axis=0, tiled=True)  6.74 us
    reduce_scatter x1, waiting for transfers between devices, apply_experts(): lax.psum_scatter(partial_value, 'tp', scatter_dimension=3, tiled=True)  4.12 us
    dot_general x1, matrix products, apply_experts(): jnp.einsum('sjcf,jfd->sjcd', hidden, w_down, preferred_element_type=jnp.f...  3.35 us
    psum x1, blocking collectives, local(): total_squares = lax.psum(jnp.sum(values * values, axis=-1), 'tp')  2.62 us
    dot_general x1, matrix products, local(): jnp.dot(shared_hidden, shared_down, preferred_element_type=jnp.float32)  2.6 us
    reshape x2, local copies, waits for them, and re-layouts, local(): outgoing = outgoing.reshape(n_ep, exp_dev, capacity, normed.shape[1])  2.09 us
  transfers between devices with their start and end apart: 3, of which 2 were waited for; matrix products, arithmetic and copies ran while one was open for 9% of the time, Pallas kernels for 0%

commit v1 on v0

v1 whole, which is shorter than its diff:
```python
import functools
import math

import jax
import jax.numpy as jnp
from jax import lax
from jax.experimental import pallas as pl
from jax.experimental.pallas import tpu as pltpu
from jax.sharding import PartitionSpec as P

eps = 1e-06
routed_scale = 2.5
MESH = pl.DeviceIdType.MESH
f32 = jnp.float32
bf16 = jnp.bfloat16


def kernel(
    n_ep, plane, rows, chunk,
    tok, gain, ids, gates, wg_h, wu_h, wd_h, sg_h, su_h, sd_h,
    out,
    g, wg, wu, wd, sg, su, hid, ysend, yrecv, yown, sums, r1, tsum, r2,
    wsem, zs, zr, ps, pr, ds, dr, ys, yr, rs, rr, bs, br,
):
    nz = n_ep // plane
    e = lax.axis_index("ep")
    c = lax.axis_index("tp")
    other = 1 - c
    z, q = e // plane, e % plane
    tok_dev, half = tok.shape
    exp_dev, feats, hidden = wg_h.shape
    experts = exp_dev * n_ep
    width = g.shape[3]
    tile = ysend.shape[2]
    tiles = half // tile
    chunks = n_ep * rows // chunk
    per = chunk // rows

    def ep_of(zi, qi):
        return zi * plane + qi

    z_others = [(z + d) % nz for d in range(1, nz)]
    q_others = [(q + d) % plane for d in range(1, plane)]

    barrier = pltpu.get_barrier_semaphore()
    for zi in z_others:
        pl.semaphore_signal(barrier, inc=1, device_id={"ep": ep_of(zi, q)}, device_id_type=MESH)
    for qi in q_others:
        pl.semaphore_signal(barrier, inc=1, device_id={"ep": ep_of(z, qi)}, device_id_type=MESH)
    pl.semaphore_signal(barrier, inc=1, device_id={"tp": other}, device_id_type=MESH)

    loads = [
        pltpu.make_async_copy(sg_h, sg, wsem.at[0]),
        pltpu.make_async_copy(su_h, su, wsem.at[1]),
        pltpu.make_async_copy(wg_h, wg, wsem.at[2]),
        pltpu.make_async_copy(wu_h, wu, wsem.at[3]),
        pltpu.make_async_copy(sd_h, wd.at[pl.ds(exp_dev * hidden, hidden)], wsem.at[4]),
    ]
    for j in range(exp_dev):
        loads.append(
            pltpu.make_async_copy(wd_h.at[j], wd.at[pl.ds(j * hidden, hidden)], wsem.at[5 + j])
        )
    for load in loads:
        load.start()

    values = tok[...].astype(f32)
    squares = jnp.sum(values * values, axis=-1, keepdims=True)
    weight = gates[...] / jnp.sum(gates[...], axis=-1, keepdims=True) * routed_scale
    lane = lax.broadcasted_iota(jnp.int32, (tok_dev, width - half), 1)
    dense = jnp.zeros((tok_dev, width - half), f32)
    chosen = ids[...]
    for k in range(chosen.shape[1]):
        dense += jnp.where(lane == chosen[:, k : k + 1], weight[:, k : k + 1], 0.0)
    dense_hi = dense.astype(bf16).astype(f32)
    extra = jnp.where(c == 0, dense_hi, dense - dense_hi)
    sq_a = squares.astype(bf16).astype(f32)
    sq_b = (squares - sq_a).astype(bf16).astype(f32)
    sq_c = squares - sq_a - sq_b
    extra = jnp.where(lane == experts, sq_a, extra)
    extra = jnp.where(lane == experts + 1, sq_b, extra)
    extra = jnp.where(lane == experts + 2, sq_c, extra)
    g[c, e] = jnp.zeros((rows, width), bf16)
    g[c, e, :tok_dev, :half] = (values * gain[...].astype(f32)).astype(bf16)
    g[c, e, :tok_dev, half:] = extra.astype(bf16)
    hid[:, exp_dev * hidden :] = jnp.zeros((hid.shape[0], hidden), bf16)

    pl.semaphore_wait(barrier, (nz - 1) + (plane - 1) + 1)

    def z_copy(zi):
        return pltpu.make_async_remote_copy(
            src_ref=g.at[c, e], dst_ref=g.at[c, e], send_sem=zs.at[zi], recv_sem=zr.at[z],
            device_id={"ep": ep_of(zi, q)}, device_id_type=MESH)

    def z_arrival(zi):
        piece = g.at[c, ep_of(zi, q)]
        return pltpu.make_async_remote_copy(
            src_ref=piece, dst_ref=piece, send_sem=zs.at[zi], recv_sem=zr.at[zi],
            device_id={"ep": ep_of(zi, q)}, device_id_type=MESH)

    def plane_copy(zi, qi):
        piece = g.at[c, ep_of(zi, q)]
        return pltpu.make_async_remote_copy(
            src_ref=piece, dst_ref=piece, send_sem=ps.at[qi, zi], recv_sem=pr.at[q, zi],
            device_id={"ep": ep_of(z, qi)}, device_id_type=MESH)

    def plane_arrival(zi, qi):
        piece = g.at[c, ep_of(zi, qi)]
        return pltpu.make_async_remote_copy(
            src_ref=piece, dst_ref=piece, send_sem=ps.at[qi, zi], recv_sem=pr.at[qi, zi],
            device_id={"ep": ep_of(z, qi)}, device_id_type=MESH)

    def partner_copy(ei):
        piece = g.at[c, ei]
        return pltpu.make_async_remote_copy(
            src_ref=piece, dst_ref=piece, send_sem=ds.at[ei], recv_sem=dr.at[ei],
            device_id={"tp": other}, device_id_type=MESH)

    def partner_arrival(ei):
        piece = g.at[other, ei]
        return pltpu.make_async_remote_copy(
            src_ref=piece, dst_ref=piece, send_sem=ds.at[ei], recv_sem=dr.at[ei],
            device_id={"tp": other}, device_id_type=MESH)

    for zi in z_others:
        z_copy(zi).start()
    for qi in q_others:
        plane_copy(z, qi).start()
    partner_copy(e).start()

    for zi in z_others:
        z_arrival(zi).wait_recv()
        for qi in q_others:
            plane_copy(zi, qi).start()
        partner_copy(ep_of(zi, q)).start()

    def row_scale(extras):
        lanes = lax.broadcasted_iota(jnp.int32, extras.shape, 1)
        inside = (lanes >= experts) & (lanes < experts + 3)
        total = jnp.sum(jnp.where(inside, extras, 0.0), axis=-1, keepdims=True)
        return lax.rsqrt(total / feats + eps)

    def gated(gate_value, up_value, scale):
        gate_value, up_value = gate_value * scale, up_value * scale
        return gate_value / (1.0 + jnp.exp(-gate_value)) * up_value

    partner_arrival(e).wait_recv()
    loads[0].wait()
    loads[1].wait()
    own_0, own_1 = g[0, e], g[1, e]
    scale = row_scale(own_0[:, half:].astype(f32) + own_1[:, half:].astype(f32))
    gate_value = jnp.dot(own_0[:, :half], sg[:half], preferred_element_type=f32)
    gate_value += jnp.dot(own_1[:, :half], sg[half:], preferred_element_type=f32)
    up_value = jnp.dot(own_0[:, :half], su[:half], preferred_element_type=f32)
    up_value += jnp.dot(own_1[:, :half], su[half:], preferred_element_type=f32)
    hid[pl.ds(pl.multiple_of(e * rows, rows), rows), exp_dev * hidden :] = gated(
        gate_value, up_value, scale).astype(bf16)

    for zi in [z] + z_others:
        for qi in q_others:
            plane_arrival(zi, qi).wait_recv()
            partner_copy(ep_of(zi, qi)).start()
    for zi in z_others:
        partner_arrival(ep_of(zi, q)).wait_recv()
    for zi in [z] + z_others:
        for qi in q_others:
            partner_arrival(ep_of(zi, qi)).wait_recv()
    for load in loads[2:]:
        load.wait()

    def partner_tile(m, n):
        return pltpu.make_async_remote_copy(
            src_ref=ysend.at[n, pl.ds(m * chunk, chunk)], dst_ref=yrecv.at[n, pl.ds(m * chunk, chunk)],
            send_sem=ys.at[m, n], recv_sem=yr.at[m, n],
            device_id={"tp": other}, device_id_type=MESH)

    def compute(m, carry):
        first = pl.multiple_of(m * chunk, chunk)
        block_0 = g[0, pl.ds(m * per, per)].reshape(chunk, width)
        block_1 = g[1, pl.ds(m * per, per)].reshape(chunk, width)
        x_0, x_1 = block_0[:, :half], block_1[:, :half]
        extras = block_0[:, half:].astype(f32) + block_1[:, half:].astype(f32)
        scale = row_scale(extras)
        lanes = lax.broadcasted_iota(jnp.int32, extras.shape, 1)
        for j in range(exp_dev):
            weights = jnp.sum(jnp.where(lanes == e * exp_dev + j, extras, 0.0), axis=-1, keepdims=True)
            gate_value = jnp.dot(x_0, wg[j, :half], preferred_element_type=f32)
            gate_value += jnp.dot(x_1, wg[j, half:], preferred_element_type=f32)
            up_value = jnp.dot(x_0, wu[j, :half], preferred_element_type=f32)
            up_value += jnp.dot(x_1, wu[j, half:], preferred_element_type=f32)
            hid[pl.ds(first, chunk), j * hidden : (j + 1) * hidden] = (
                gated(gate_value, up_value, scale) * weights).astype(bf16)
        h = hid[pl.ds(first, chunk)]
        for n in range(tiles):
            columns = pl.ds(pl.multiple_of(other * half + n * tile, tile), tile)
            ysend[n, pl.ds(first, chunk)] = jnp.dot(
                h, wd[:, columns], preferred_element_type=f32).astype(bf16)
            partner_tile(m, n).start()
        for n in range(tiles):
            columns = pl.ds(pl.multiple_of(c * half + n * tile, tile), tile)
            yown[n, pl.ds(first, chunk)] = jnp.dot(h, wd[:, columns], preferred_element_type=f32)
        return carry

    lax.fori_loop(0, chunks, compute, 0)

    def add_partner(m, carry):
        first = pl.multiple_of(m * chunk, chunk)
        for n in range(tiles):
            partner_tile(m, n).wait_recv()
            total = yown[n, pl.ds(first, chunk)] + yrecv[n, pl.ds(first, chunk)].astype(f32)
            sums[pl.ds(m * per, per), :, n * tile : (n + 1) * tile] = total.astype(bf16).reshape(
                per, rows, tile)
        return carry

    lax.fori_loop(0, chunks, add_partner, 0)

    def plane_sum(zi, qi):
        return pltpu.make_async_remote_copy(
            src_ref=sums.at[ep_of(zi, qi)], dst_ref=r1.at[q, zi], send_sem=rs.at[qi, zi],
            recv_sem=rr.at[q, zi], device_id={"ep": ep_of(z, qi)}, device_id_type=MESH)

    def plane_sum_arrival(zi, qi):
        return pltpu.make_async_remote_copy(
            src_ref=sums.at[ep_of(zi, qi)], dst_ref=r1.at[qi, zi], send_sem=rs.at[qi, zi],
            recv_sem=rr.at[qi, zi], device_id={"ep": ep_of(z, qi)}, device_id_type=MESH)

    def z_sum(zi):
        return pltpu.make_async_remote_copy(
            src_ref=tsum.at[zi], dst_ref=r2.at[z], send_sem=bs.at[zi], recv_sem=br.at[z],
            device_id={"ep": ep_of(zi, q)}, device_id_type=MESH)

    def z_sum_arrival(zi):
        return pltpu.make_async_remote_copy(
            src_ref=tsum.at[zi], dst_ref=r2.at[zi], send_sem=bs.at[zi], recv_sem=br.at[zi],
            device_id={"ep": ep_of(zi, q)}, device_id_type=MESH)

    for zi in z_others + [z]:
        for qi in q_others:
            plane_sum(zi, qi).start()
    total = None
    for zi in z_others + [z]:
        total = sums[ep_of(zi, q)].astype(f32)
        for qi in q_others:
            plane_sum_arrival(zi, qi).wait_recv()
            total += r1[qi, zi].astype(f32)
        if zi is not z:
            tsum[zi] = total.astype(bf16)
            z_sum(zi).start()
    for zi in z_others:
        z_sum_arrival(zi).wait_recv()
        total += r2[zi].astype(f32)
    out[...] = total[:tok_dev].astype(bf16)

    for zi in z_others:
        z_copy(zi).wait_send()
        z_sum(zi).wait_send()
    for zi in [z] + z_others:
        for qi in q_others:
            plane_copy(zi, qi).wait_send()
            plane_sum(zi, qi).wait_send()
            partner_copy(ep_of(zi, qi)).wait_send()
        partner_copy(ep_of(zi, q)).wait_send()

    def finish(m, carry):
        for n in range(tiles):
            partner_tile(m, n).wait_send()
        return carry

    lax.fori_loop(0, chunks, finish, 0)


def local(tokens, norm_gain, expert_ids, route_gate, w_gate, w_up, w_down, shared_gate, shared_up, shared_down):
    n_ep = lax.axis_size("ep")
    tok_dev, half = tokens.shape
    exp_dev, feats, hidden = w_gate.shape
    plane = math.gcd(n_ep, 2 ** (int(math.log2(n_ep)) // 2))
    nz = n_ep // plane
    rows = -(-tok_dev // 16) * 16
    total_rows = n_ep * rows
    chunk = rows * math.gcd(n_ep, max(1, 256 // rows))
    chunks = total_rows // chunk
    tile = min(512, half)
    tiles = half // tile
    width = half + -(-(exp_dev * n_ep + 3) // 128) * 128
    vmem = pl.BlockSpec(memory_space=pltpu.VMEM)
    anywhere = pl.BlockSpec(memory_space=pl.ANY)
    dma = pltpu.SemaphoreType.DMA
    k_rows = (exp_dev + 1) * hidden
    return pl.pallas_call(
        functools.partial(kernel, n_ep, plane, rows, chunk),
        out_shape=jax.ShapeDtypeStruct((tok_dev, half), bf16),
        in_specs=[vmem] * 4 + [anywhere] * 6,
        out_specs=vmem,
        scratch_shapes=[
            pltpu.VMEM((2, n_ep, rows, width), bf16),
            pltpu.VMEM(w_gate.shape, bf16),
            pltpu.VMEM(w_up.shape, bf16),
            pltpu.VMEM((k_rows, feats), bf16),
            pltpu.VMEM(shared_gate.shape, bf16),
            pltpu.VMEM(shared_up.shape, bf16),
            pltpu.VMEM((total_rows, k_rows), bf16),
            pltpu.VMEM((tiles, total_rows, tile), bf16),
            pltpu.VMEM((tiles, total_rows, tile), bf16),
            pltpu.VMEM((tiles, total_rows, tile), f32),
            pltpu.VMEM((n_ep, rows, half), bf16),
            pltpu.VMEM((plane, nz, rows, half), bf16),
            pltpu.VMEM((nz, rows, half), bf16),
            pltpu.VMEM((nz, rows, half), bf16),
            dma((5 + exp_dev,)),
            dma((nz,)), dma((nz,)),
            dma((plane, nz)), dma((plane, nz)),
            dma((n_ep,)), dma((n_ep,)),
            dma((chunks, tiles)), dma((chunks, tiles)),
            dma((plane, nz)), dma((plane, nz)),
            dma((nz,)), dma((nz,)),
        ],
        compiler_params=pltpu.CompilerParams(
            collective_id=0, has_side_effects=True, vmem_limit_bytes=64 * 1024 * 1024 - 131072),
    )(tokens, norm_gain.reshape(1, half), expert_ids, route_gate, w_gate, w_up, w_down,
      shared_gate, shared_up, shared_down)


def solution(mesh):
    in_specs = (
        P("ep", "tp"),
        P("tp"),
        P("ep", None),
        P("ep", None),
        P("ep", None, "tp"),
        P("ep", None, "tp"),
        P("ep", "tp", None),
        P(None, "tp"),
        P(None, "tp"),
        P("tp", None),
    )
    out_specs = P("ep", "tp")
    return jax.shard_map(local, mesh=mesh, in_specs=in_specs, out_specs=out_specs, check_vma=False)
```

time: 86.1 us -> 37.5 us (0.44)
  Pallas kernels: 0 us -> 31.8 us
  blocking collectives: 31.5 us -> 0 us
  between operations: 13.5 us -> 0.01 us
  waiting for transfers between devices: 11 us -> 0 us
  matrix products: 9.17 us -> 0 us
  starting transfers between devices: 6.78 us -> 0 us
  other arithmetic: 6.44 us -> 0 us
  local copies, waits for them, and re-layouts: 6.95 us -> 5.36 us
    pallas_call x0 -> x1, Pallas kernels: none -> 31.8 us  [local(): pl.pallas_call(functools.partial(kernel, n_ep, plane, rows, chunk), out_s...]
    all_to_all x1 -> x0, blocking collectives: 27.1 us -> none  [local(): lax.all_to_all(outgoing, 'ep', split_axis=0, concat_axis=0, tiled=True)]
    dot_general x5 -> x0, matrix products: 9.17 us -> none  [the longest x1 3.35 us: apply_experts(): jnp.einsum('sjcf,jfd->sjcd', hidden, w_down, preferred_element_type=jnp.f...]
    all_to_all x1 -> x0, waiting for transfers between devices: 6.86 us -> none  [send_back(): lax.all_to_all(results, 'ep', split_axis=0, concat_axis=0, tiled=True)]
    all_to_all x1 -> x0, starting transfers between devices: 6.74 us -> none  [send_back(): lax.all_to_all(results, 'ep', split_axis=0, concat_axis=0, tiled=True)]
    reduce_scatter x2 -> x0, waiting for transfers between devices: 4.14 us -> none  [the longest x1 4.12 us: apply_experts(): lax.psum_scatter(partial_value, 'tp', scatter_dimension=3, tiled=True)]
    unnamed x7 -> x3, local copies, waits for them, and re-layouts: 0.78 us -> 4.09 us
    convert_element_type x3 -> x0, other arithmetic: 2.91 us -> none  [the longest x1 1.38 us: local(): return (routed + shared).astype(jnp.bfloat16)]
  transfers between devices with their start and end apart: 3 -> 0, of which waited for: 2 -> 0; matrix products, arithmetic and copies ran while one was open for 9% -> 0% of each run, Pallas kernels for 0% -> 0%
where the time goes in v1:
time: 37.5 us; the launch traced here: 37.1 us
  Pallas kernels  31.8 us (85%)
  local copies, waits for them, and re-layouts  5.36 us (14%)
    pallas_call x1, Pallas kernels, local(): pl.pallas_call(functools.partial(kernel, n_ep, plane, rows, chunk), out_s...  31.8 us
    unnamed x3, local copies, waits for them, and re-layouts  4.09 us
    reshape x1, local copies, waits for them, and re-layouts, local(): norm_gain.reshape(1, half)  1.28 us

profile of v1, /device:TPU:0, one launch (start us, length us, event | category | flops | bytes accessed | tf_op | source)
XLA Modules:
  0.0 37.1 jit_solution(15621001584058405112)
XLA Ops:
  0.0 1.3 %reshape.3.gain = bf16[1,1024]{1,0:T(2,128)(2,1)} reshape(bf16[1024]{0:T(1024)(128)(2,1)} %param.11) | data formatting | bytes 4096 | tf_op jit(solution)/shard_map/reshape | solution.py:318
  1.3 1.4 %copy.11.ids = s32[12,8]{1,0:T(8,128)} copy(s32[12,8]{0,1:T(8,128)} %param.12) | data formatting | bytes 768 | tf_op args[2]
  2.6 1.4 %copy.12.gates = f32[12,8]{1,0:T(8,128)} copy(f32[12,8]{0,1:T(8,128)} %param.13) | data formatting | bytes 768 | tf_op args[3]
  4.0 31.8 %shard_map.100 = bf16[12,1024]{1,0:T(8,128)(2,1)} custom-call(bf16[12,1024]{1,0:T(8,128)(2,1)} %tok.1, bf16[1,1024]{1,0:T(2,128)(2,1)} %reshape.3.gain, s32[12,8]{1,0:T(8,128)} %copy.11.ids, f32[12,8]{1,0:T(8,128)} %copy.12.gates, bf16[2,2048,256]{2,1,0:T(8,128)(2,1)} %wg_h.1, bf16[2,2048,256]{2,1,0:T(8,128)(2,1)} %wu_h.1, bf16[2,256,2048]{2,1,0:T(8,128)(2,1)} %wd_h.1, ...), custom_call_target="tpu_custom_call" | custom-call | tf_op jit(solution)/shard_map/pallas_call | solution.py:288
  35.8 1.4 %copy.14 = bf16[12,1024]{1,0:T(8,128)(2,1)} copy(bf16[12,1024]{1,0:T(8,128)(2,1)} %shard_map.100) | data formatting | bytes 49152
